TPU v7x, 32 devices: a whole 2x2x4 slice. The times are simulated.
32 devices in a mesh: gr: 2 (over x), fs: 4 (over z), tp: 4 (over y, core).
Axes of the slice: x: 2, y: 2, z: 4, core: 2. Of those that a mesh axis runs over, the one named last changes fastest.
Arguments:
- prompt: bfloat16 [4096, 2048], P(('gr', 'fs', 'tp')), may hold values from -6 to 6
- train_gate: float32 [16, 2048, 256], P(None, ('gr', 'fs'), 'tp'), may hold values from -0.125 to 0.125
- train_up: float32 [16, 2048, 256], P(None, ('gr', 'fs'), 'tp'), may hold values from -0.125 to 0.125
- train_down: float32 [16, 256, 2048], P(None, 'tp', ('gr', 'fs')), may hold values from -0.375 to 0.375
- train_shared_gate: float32 [2048, 256], P(('gr', 'fs'), 'tp'), may hold values from -0.125 to 0.125
- train_shared_up: float32 [2048, 256], P(('gr', 'fs'), 'tp'), may hold values from -0.125 to 0.125
- train_shared_down: float32 [256, 2048], P('tp', ('gr', 'fs')), may hold values from -0.375 to 0.375
- norm_gain: float32 [2048], P(('gr', 'fs')), may hold values from 0.1 to 1.9
- expert_ids: int32 [4096, 8], P(('gr', 'fs', 'tp')), may hold values from 0 to 15, all different within a row; in each aligned block of 128 rows (0 to 127, 128 to 255, ...) at most 65 rows name the same one
- route_weight: float32 [4096, 8], P(('gr', 'fs', 'tp')), may hold values from 0.05 to 0.6
Outputs:
- serve_gate: bfloat16 [16, 2048, 256], P(('fs', 'tp'))
- serve_up: bfloat16 [16, 2048, 256], P(('fs', 'tp'))
- serve_down: bfloat16 [16, 256, 2048], P(('fs', 'tp'))
- serve_shared_gate: bfloat16 [2048, 256], P(None, 'tp')
- serve_shared_up: bfloat16 [2048, 256], P(None, 'tp')
- serve_shared_down: bfloat16 [256, 2048], P('tp')
- mixed_out: bfloat16 [4096, 2048], P(('gr', 'fs', 'tp'))
Inputs may be any that keep to these rules, and one draw needn't show every extreme that they name: `expert_ids`: each row names 8 different experts. Among the rows of one device no expert is named by more than 65 rows, and in some device's rows one expert is named by exactly 65.
All inputs are finite; a program needn't handle non-finite values.
Results may differ from a plain program's by a relative error of at most 0.012.
Values may be sent and summed in bfloat16 or wider, within the bound.
No kernel may reach another device: no remote copies, remote signals or barrier semaphores. Data moves between devices by JAX's collectives and lax.ppermute only.
A program may use at most 128 MiB of HBM per device.

v0:
```python
import jax
import jax.numpy as jnp
from jax import lax
from jax.sharding import PartitionSpec as P

eps_norm = 1e-06
row_tile = 8


def to_owners(pieces):
    count, kinds, hidden_part, width_part = pieces.shape
    fs, tp = (lax.axis_size("fs"), lax.axis_size("tp"))
    pieces = lax.all_to_all(pieces, ("fs", "tp"), split_axis=0, concat_axis=0, tiled=True)
    pieces = pieces.reshape(fs, tp, kinds, hidden_part, width_part)
    pieces = pieces.transpose(2, 1, 3, 0, 4).reshape(kinds, tp * hidden_part, fs * width_part)
    return lax.all_gather(pieces, "gr", axis=2, tiled=True)


def dot_last(left, right):
    return lax.dot_general(
        left, right, (((1,), (1,)), ((), ())), preferred_element_type=jnp.float32
    )


def gated(rows, gate_up):
    both = dot_last(rows, gate_up)
    hidden = both.shape[1] // 2
    return jax.nn.silu(both[:, :hidden]) * both[:, hidden:]


def dense_mix(normed, expert_ids, route_weight, gate_up, lowered, shared_gate_up, shared_down):
    fs, tp = (lax.axis_size("fs"), lax.axis_size("tp"))
    expert_count = fs * tp
    row_count, model_width = normed.shape
    named = expert_ids[None, :, :] == jnp.arange(expert_count, dtype=jnp.int32)[:, None, None]
    weights = jnp.sum(jnp.where(named, route_weight[None], 0.0), axis=2)
    high = lax.reduce_precision(weights, 8, 7)
    coded = jnp.stack((high, weights - high)).astype(jnp.bfloat16).reshape(-1)
    extra = -(-coded.size // (model_width * row_tile)) * row_tile
    coded = jnp.pad(coded, (0, extra * model_width - coded.size)).reshape(extra, model_width)
    block = lax.all_gather(jnp.concatenate((normed, coded), axis=0), ("fs", "tp"), axis=0)
    height = row_count + extra
    mine = lax.axis_index("fs") * tp + lax.axis_index("tp")
    sent = block[:, row_count:].reshape(expert_count, -1)[:, : 2 * expert_count * row_count]
    sent = sent.reshape(expert_count, 2, expert_count, row_count)
    own = lax.dynamic_index_in_dim(sent, mine, axis=2, keepdims=False).astype(jnp.float32)
    own = (own[:, 0] + own[:, 1])[:, :, None]
    act = gated(block.reshape(-1, model_width), gate_up).reshape(expert_count, height, -1)
    act = (act[:, :row_count] * own).astype(jnp.bfloat16)
    near = lax.dynamic_slice_in_dim(block, lax.axis_index("fs") * tp, tp, axis=0)
    shared_act = gated(near.reshape(-1, model_width), shared_gate_up).astype(jnp.bfloat16)
    shared_act = shared_act.reshape(tp, height, -1)[:, :row_count]
    placed = jnp.zeros((expert_count, row_count, shared_act.shape[2]), jnp.bfloat16)
    placed = lax.dynamic_update_slice_in_dim(placed, shared_act, lax.axis_index("fs") * tp, axis=0)
    act = jnp.concatenate((act, placed), axis=2).reshape(expert_count * row_count, -1)
    down = jnp.concatenate((lowered, shared_down), axis=0)
    partial = jnp.dot(act, down, preferred_element_type=jnp.float32).astype(jnp.bfloat16)
    return lax.psum_scatter(partial, ("fs", "tp"), scatter_dimension=0, tiled=True)


def sparse_mix(normed, expert_ids, route_weight, gate_up, lowered, shared_gate_up, shared_down):
    block_rows = lax.all_gather(normed, "tp", axis=0, tiled=True)
    shared_act = gated(block_rows, shared_gate_up).astype(jnp.bfloat16)
    shared_sum = lax.psum_scatter(
        jnp.dot(shared_act, shared_down, preferred_element_type=jnp.float32).astype(jnp.bfloat16),
        "tp",
        scatter_dimension=0,
        tiled=True,
    ).astype(jnp.float32)
    row_count, model_width = normed.shape
    top_count = expert_ids.shape[1]
    expert_count = lax.axis_size("fs") * lax.axis_size("tp")
    capacity = row_count * top_count // expert_count + 1
    flat_ids = expert_ids.reshape(-1)
    onehot = (flat_ids[:, None] == jnp.arange(expert_count, dtype=jnp.int32)[None, :]).astype(
        jnp.int32
    )
    earlier = jnp.cumsum(onehot, axis=0) - onehot
    places = jnp.sum(earlier * onehot, axis=1)
    slot_ids = (flat_ids * capacity + places).reshape(row_count, top_count)
    slot_range = jnp.arange(expert_count * capacity, dtype=jnp.int32)
    dispatch = jnp.any(slot_range[:, None, None] == slot_ids[None, :, :], axis=-1).astype(
        jnp.bfloat16
    )
    outgoing = jnp.dot(dispatch, normed, preferred_element_type=jnp.float32).astype(jnp.bfloat16)
    outgoing = outgoing.reshape(expert_count, capacity, model_width)
    arrived = lax.all_to_all(outgoing, ("fs", "tp"), split_axis=0, concat_axis=0, tiled=True)
    source_count, slot_count, width_here = arrived.shape
    arrived_rows = arrived.reshape(source_count * slot_count, width_here)
    hidden = gated(arrived_rows, gate_up).astype(jnp.bfloat16)
    result = jnp.dot(hidden, lowered, preferred_element_type=jnp.float32).astype(jnp.bfloat16)
    result = result.reshape(source_count, slot_count, width_here)
    returned = lax.all_to_all(result, ("fs", "tp"), split_axis=0, concat_axis=0, tiled=True)
    picked = returned.reshape(expert_count * capacity, model_width)[slot_ids]
    routed = jnp.sum(route_weight[:, :, None] * picked.astype(jnp.float32), axis=1)
    return (routed + shared_sum).astype(jnp.bfloat16)


def body(
    prompt,
    train_gate,
    train_up,
    train_down,
    train_shared_gate,
    train_shared_up,
    train_shared_down,
    norm_gain,
    expert_ids,
    route_weight,
):
    widened = prompt.astype(jnp.float32)
    normed = (
        widened * lax.rsqrt(jnp.mean(widened * widened, axis=-1, keepdims=True) + eps_norm)
    ).astype(jnp.bfloat16)
    gained_gate = jnp.swapaxes(train_gate, 1, 2) * norm_gain
    gained_up = jnp.swapaxes(train_up, 1, 2) * norm_gain
    stacked = to_owners(jnp.stack((gained_gate, gained_up), axis=1).astype(jnp.bfloat16))
    lowered = to_owners(train_down.astype(jnp.bfloat16)[:, None])
    shared = jnp.stack(
        (
            train_shared_gate.T * norm_gain,
            train_shared_up.T * norm_gain,
            train_shared_down,
            jnp.zeros_like(train_shared_down),
        )
    ).astype(jnp.bfloat16)
    shared = lax.all_gather(shared, ("gr", "fs"), axis=0)
    shared = shared[:, :3].transpose(1, 2, 0, 3).reshape(3, train_shared_down.shape[0], -1)
    model_width = prompt.shape[1]
    mix = (
        dense_mix
        if lax.axis_size("fs") * lax.axis_size("tp") <= 2 * expert_ids.shape[1]
        else sparse_mix
    )
    mixed_out = mix(
        normed,
        expert_ids,
        route_weight,
        stacked.reshape(-1, model_width),
        lowered[0],
        shared[:2].reshape(-1, model_width),
        shared[2],
    )
    return (
        jnp.swapaxes(stacked[:1], 1, 2),
        jnp.swapaxes(stacked[1:], 1, 2),
        lowered,
        shared[0].T,
        shared[1].T,
        shared[2],
        mixed_out,
    )


def solution(mesh):
    placed = (
        P(("gr", "fs", "tp"), None),
        P(None, ("gr", "fs"), "tp"),
        P(None, ("gr", "fs"), "tp"),
        P(None, "tp", ("gr", "fs")),
        P(("gr", "fs"), "tp"),
        P(("gr", "fs"), "tp"),
        P("tp", ("gr", "fs")),
        P(("gr", "fs")),
        P(("gr", "fs", "tp"), None),
        P(("gr", "fs", "tp"), None),
    )
    return jax.shard_map(
        body,
        mesh=mesh,
        in_specs=placed,
        out_specs=(
            P(("fs", "tp"), None, None),
            P(("fs", "tp"), None, None),
            P(("fs", "tp"), None, None),
            P(None, "tp"),
            P(None, "tp"),
            P("tp", None),
            P(("gr", "fs", "tp"), None),
        ),
        check_vma=False,
    )
```

profile of v0, /device:TPU:0, one launch (start us, length us, event | category | flops | bytes accessed | tf_op | source)
XLA Modules:
  0.0 323.8 jit_solution(4078553129348858008)
XLA Ops:
  7.2 1.0 convert_bitcast_fusion.1
  8.3 0.9 fusion.9
  10.8 1.2 fusion.4
  12.1 1.2 fusion.5
  13.3 0.9 pad_maximum_fusion.2
  14.6 43.9 %all_to_all.10 = bf16[16,2,64,256]{3,2,1,0:T(8,128)(2,1)S(1)} all-to-all(bf16[16,2,64,256]{3,2,1,0:T(8,128)(2,1)S(1)} %pad_maximum_fusion.1), channel_id=1, replica_groups=mesh['gr'=2,'fs'=4,'tp'=4] {'fs','tp'}, dimensions={0} | all-to-all | bytes 2097152 | tf_op jit(solution)/shard_map/all_to_all | solution.py:13
  59.3 1.5 reshape.162
  60.9 0.9 convert_bitcast_fusion
  61.7 5.1 %all-to-all-start.1 = ((bf16[16,1,64,256]{3,2,1,0:T(8,128)(2,1)}), bf16[16,1,64,256]{3,2,1,0:T(8,128)(2,1)S(1)}, u32[]{:S(2)}, u32[]{:S(2)}) async-start(bf16[16,1,64,256]{3,2,1,0:T(8,128)(2,1)} %convert_bitcast_fusion), calls=%async_computation.1 | async-start | bytes 1048576 | tf_op jit(solution)/shard_map/all_to_all | solution.py:13
  66.9 21.5 %all-to-all-done.1 = bf16[16,1,64,256]{3,2,1,0:T(8,128)(2,1)S(1)} async-done(((bf16[16,1,64,256]{3,2,1,0:T(8,128)(2,1)}), bf16[16,1,64,256]{3,2,1,0:T(8,128)(2,1)S(1)}, u32[]{:S(2)}, u32[]{:S(2)}) %all-to-all-start.1) | async-done | bytes 524320 | tf_op jit(solution)/shard_map/all_to_all | solution.py:13
  88.8 1.2 reshape.164
  90.1 1.2 slice_bitcast_fusion.2
  91.8 55.9 %all-gather.12.cloned.1.call-done = bf16[2176,2048]{1,0:T(8,128)(2,1)} async-done(((bf16[136,2048]{1,0:T(8,128)(2,1)}), bf16[2176,2048]{1,0:T(8,128)(2,1)}) %all-gather.12.cloned.1.call-update) | async-done | bytes 8912912 | tf_op jit(solution)/shard_map/all_gather | solution.py:41
  147.7 1.1 slice.82
  148.8 1.8 constant_dynamic-slice_fusion
  152.1 29.4 %all-gather.6.cloned.1.call-done = bf16[2,256,2048]{2,1,0:T(8,128)(2,1)} async-done(((bf16[2,256,1024]{2,1,0:T(8,128)(2,1)}), bf16[2,256,2048]{2,1,0:T(8,128)(2,1)}) %all-gather.6.cloned.1.call-update) | async-done | bytes 2097168 | tf_op jit(solution)/shard_map/all_gather | solution.py:16
  181.5 8.0 %fusion.14 = f32[2176,512]{1,0:T(8,128)S(1)} fusion(bf16[2176,2048]{1,0:T(8,128)(2,1)} %all-gather.12.cloned.1.call-done, bf16[512,2048]{1,0:T(8,128)(2,1)} %bitcast.84), kind=kOutput, calls=%fused_computation.45 | convolution fusion | flops 4563402752 | bytes 15466496 | tf_op jit(solution)/shard_map/dot_general | solution.py:20
  190.7 14.1 %all-gather.8.cloned.1.call-done = bf16[1,256,2048]{2,1,0:T(8,128)(2,1)} async-done(((bf16[1,256,1024]{2,1,0:T(8,128)(2,1)}), bf16[1,256,2048]{2,1,0:T(8,128)(2,1)}) %all-gather.8.cloned.1.call-update) | async-done | bytes 1048592 | tf_op jit(solution)/shard_map/all_gather | solution.py:16
  204.8 7.9 %convolution_convert_fusion = bf16[2048,2048]{1,0:T(8,128)(2,1)} fusion(bf16[2048,320]{1,0:T(8,128)(2,1)S(1)} %bitcast.88, bf16[64,2048]{1,0:T(8,128)(2,1)S(1)} %bitcast.97, bf16[256,2048]{1,0:T(8,128)(2,1)} %bitcast.89), kind=kOutput, calls=%fused_computation | convolution fusion | flops 2691170304 | bytes 11010048 | tf_op jit(solution)/shard_map/dot_general | solution.py:57
  214.1 1.7 slice_bitcast_fusion
  215.8 1.3 copy.60
  217.1 1.3 copy.61
  218.4 97.8 %reduce-scatter.2.cloned.1.call-done = bf16[128,2048]{1,0:T(8,128)(2,1)} async-done(((bf16[2048,2048]{1,0:T(8,128)(2,1)}), bf16[128,2048]{1,0:T(8,128)(2,1)}) %reduce-scatter.2.cloned.1.call-update) | async-done | bytes 524304 | tf_op jit(solution)/shard_map/reduce_scatter | solution.py:58
  316.3 1.0 copy.75
  (54 shorter events, 8.0 us)
Async XLA Ops:
  7.2 7.0 %copy-start.5 = (f32[256]{0:T(256)S(1)}, f32[256]{0:T(256)}, u32[]{:S(2)}) copy-start(f32[256]{0:T(256)} %param.17) | copy-start | bytes 3076
  7.2 7.0 %copy-start.1 = (f32[16,256,64]{1,2,0:T(8,128)S(1)}, f32[16,256,64]{1,2,0:T(8,128)}, u32[]{:S(2)}) copy-start(f32[16,256,64]{1,2,0:T(8,128)} %param.11) | copy-start | bytes 3145732
  7.2 7.0 %copy-start.2 = (f32[16,256,64]{1,2,0:T(8,128)S(1)}, f32[16,256,64]{1,2,0:T(8,128)}, u32[]{:S(2)}) copy-start(f32[16,256,64]{1,2,0:T(8,128)} %param.12) | copy-start | bytes 3145732
  7.2 82.9 %all-gather.10.cloned.1.call-start = ((), (), s32[]{:S(2)}) async-start(), calls=%async_computation.5 | async-start | bytes 1179648 | tf_op jit(solution)/shard_map/all_gather | solution.py:127
  10.0 137.8 %all-gather.12.cloned.1.call-start = ((), (), s32[]{:S(2)}) async-start(), calls=%async_computation.7 | async-start | bytes 9469952 | tf_op jit(solution)/shard_map/all_gather | solution.py:41
  14.1 167.3 %all-gather.6.cloned.1.call-start = ((), (), s32[]{:S(2)}) async-start(), calls=%async_computation.3 | async-start | bytes 3145728 | tf_op jit(solution)/shard_map/all_gather | solution.py:16
  58.5 2.4 copy-start
  61.7 26.7 %all-to-all-start.1 = ((bf16[16,1,64,256]{3,2,1,0:T(8,128)(2,1)}), bf16[16,1,64,256]{3,2,1,0:T(8,128)(2,1)S(1)}, u32[]{:S(2)}, u32[]{:S(2)}) async-start(bf16[16,1,64,256]{3,2,1,0:T(8,128)(2,1)} %convert_bitcast_fusion), calls=%async_computation.1 | async-start | bytes 1048576 | tf_op jit(solution)/shard_map/all_to_all | solution.py:13
  66.8 137.9 %all-gather.8.cloned.1.call-start = ((), (), s32[]{:S(2)}) async-start(), calls=%async_computation.4 | async-start | bytes 1572864 | tf_op jit(solution)/shard_map/all_gather | solution.py:16
  90.0 226.3 %reduce-scatter.2.cloned.1.call-start = ((), (), s32[]{:S(2)}) async-start(), calls=%async_computation.6 | async-start | bytes 8912896 | tf_op jit(solution)/shard_map/reduce_scatter | solution.py:58
  91.8 112.9 %copy-start.4 = (bf16[8,8,8,256]{3,1,2,0:T(8,128)(2,1)}, bf16[8,8,8,256]{3,1,2,0:T(8,128)(2,1)S(1)}, u32[]{:S(2)}) copy-start(bf16[8,8,8,256]{3,1,2,0:T(8,128)(2,1)S(1)} %copy.64) | copy-start | bytes 786436
  215.8 100.5 %copy-start.3 = (bf16[1,256,2048]{2,1,0:T(8,128)(2,1)S(1)}, bf16[1,256,2048]{2,1,0:T(8,128)(2,1)}, u32[]{:S(2)}) copy-start(bf16[1,256,2048]{2,1,0:T(8,128)(2,1)} %all-gather.8.cloned.1.call-done) | copy-start | bytes 3145732
Sparse Core Ops, SparseCore 0:
  10.7 48.1 all-gather.9
  61.8 85.8 all-gather.11
  149.8 31.5 all-gather.5
  183.4 21.2 all-gather.7
  212.8 103.4 reduce-scatter.1
where the time goes:
time: 324 us
  waiting for transfers between devices  219 us (68%)
  blocking collectives  43.9 us (14%)
  matrix products  16.7 us (5%)
  local copies, waits for them, and re-layouts  15.8 us (5%)
  between operations  14.1 us (4%)
  other arithmetic  9.15 us (3%)
  starting transfers between devices  5.29 us (2%)
    reduce_scatter x1, waiting for transfers between devices, dense_mix(): lax.psum_scatter(partial, ('fs', 'tp'), scatter_dimension=0, tiled=True)  97.8 us
    all_gather x1, waiting for transfers between devices, dense_mix(): lax.all_gather(jnp.concatenate((normed, coded), axis=0), ('fs', 'tp'), ax...  55.9 us
    all_to_all x1, blocking collectives, to_owners(): lax.all_to_all(pieces, ('fs', 'tp'), split_axis=0, concat_axis=0, tiled=T...  43.9 us
    all_gather x2, waiting for transfers between devices, to_owners(): return lax.all_gather(pieces, 'gr', axis=2, tiled=True)  43.5 us
    all_to_all x1, waiting for transfers between devices, to_owners(): lax.all_to_all(pieces, ('fs', 'tp'), split_axis=0, concat_axis=0, tiled=T...  21.5 us
    dot_general x2, matrix products, dot_last(): lax.dot_general(left, right, (((1,), (1,)), ((), ())), preferred_element_...  8.8 us
    dot_general x1, matrix products, dense_mix(): jnp.dot(act, down, preferred_element_type=jnp.float32).astype(jnp.bfloat16)  7.9 us
  transfers between devices with their start and end apart: 6, of which 5 were waited for; matrix products, arithmetic and copies ran while one was open for 9% of the time, Pallas kernels for 0%

commit v1 on v0

--- a/solution.py
+++ b/solution.py
@@ -13,7 +13,7 @@
     pieces = lax.all_to_all(pieces, ("fs", "tp"), split_axis=0, concat_axis=0, tiled=True)
     pieces = pieces.reshape(fs, tp, kinds, hidden_part, width_part)
     pieces = pieces.transpose(2, 1, 3, 0, 4).reshape(kinds, tp * hidden_part, fs * width_part)
-    return lax.all_gather(pieces, "gr", axis=2, tiled=True)
+    return jnp.concatenate(lax.all_gather(pieces, "gr"), axis=2)
 
 
 def dot_last(left, right):

time: 324 us -> 337 us (1.040)
  blocking collectives: 43.9 us -> 0 us
  waiting for transfers between devices: 219 us -> 259 us
  local copies, waits for them, and re-layouts: 15.8 us -> 30.9 us
  starting transfers between devices: 5.29 us -> 12 us
  matrix products: 16.7 us -> 12.7 us
    all_to_all x1 -> x0, blocking collectives: 43.9 us -> none  [to_owners(): lax.all_to_all(pieces, ('fs', 'tp'), split_axis=0, concat_axis=0, tiled=T...]
    all_gather x1, waiting for transfers between devices: 55.9 us -> 74.6 us  [dense_mix(): lax.all_gather(jnp.concatenate((normed, coded), axis=0), ('fs', 'tp'), ax...]
    all_to_all x1 -> x2, waiting for transfers between devices: 21.5 us -> 38.2 us  [to_owners(): lax.all_to_all(pieces, ('fs', 'tp'), split_axis=0, concat_axis=0, tiled=T...]
    all_gather x2, waiting for transfers between devices: 43.5 us -> 53.2 us  [to_owners(): return jnp.concatenate(lax.all_gather(pieces, 'gr'), axis=2)]
    reduce_scatter x1, waiting for transfers between devices: 97.8 us -> 90.4 us  [dense_mix(): lax.psum_scatter(partial, ('fs', 'tp'), scatter_dimension=0, tiled=True)]
    all_to_all x1 -> x2, starting transfers between devices: 5.08 us -> 11.6 us  [to_owners(): lax.all_to_all(pieces, ('fs', 'tp'), split_axis=0, concat_axis=0, tiled=T...]
    unnamed x22 -> x35, local copies, waits for them, and re-layouts: 5.5 us -> 10.2 us
    all_gather x0 -> x2, local copies, waits for them, and re-layouts: none -> 4.1 us  [to_owners(): return jnp.concatenate(lax.all_gather(pieces, 'gr'), axis=2)]
  transfers between devices with their start and end apart: 6 -> 7, of which waited for: 5 -> 7; matrix products, arithmetic and copies ran while one was open for 9% -> 9% of each run, Pallas kernels for 0% -> 0%
where the time goes in v1:
time: 337 us; the launch traced here: 336 us
  waiting for transfers between devices  259 us (77%)
  local copies, waits for them, and re-layouts  30.9 us (9%)
  between operations  14.2 us (4%)
  matrix products  12.7 us (4%)
  starting transfers between devices  12 us (4%)
  other arithmetic  6.82 us (2%)
    reduce_scatter x1, waiting for transfers between devices, dense_mix(): lax.psum_scatter(partial, ('fs', 'tp'), scatter_dimension=0, tiled=True)  90.4 us
    all_gather x1, waiting for transfers between devices, dense_mix(): lax.all_gather(jnp.concatenate((normed, coded), axis=0), ('fs', 'tp'), ax...  74.6 us
    all_gather x2, waiting for transfers between devices, to_owners(): return jnp.concatenate(lax.all_gather(pieces, 'gr'), axis=2)  53.2 us
    all_to_all x2, waiting for transfers between devices, to_owners(): lax.all_to_all(pieces, ('fs', 'tp'), split_axis=0, concat_axis=0, tiled=T...  38.2 us
    all_to_all x2, starting transfers between devices, to_owners(): lax.all_to_all(pieces, ('fs', 'tp'), split_axis=0, concat_axis=0, tiled=T...  11.6 us
    unnamed x35, local copies, waits for them, and re-layouts  10.2 us
    dot_general x1, matrix products, dense_mix(): jnp.dot(act, down, preferred_element_type=jnp.float32).astype(jnp.bfloat16)  7.1 us
  transfers between devices with their start and end apart: 7, of which 7 were waited for; matrix products, arithmetic and copies ran while one was open for 9% of the time, Pallas kernels for 0%

profile of v1, /device:TPU:0, one launch (start us, length us, event | category | flops | bytes accessed | tf_op | source)
XLA Modules:
  0.0 336.1 jit_solution(124361531711967149)
XLA Ops:
  7.2 2.2 convert_bitcast_fusion
  9.5 7.4 %all-to-all-start.1 = ((bf16[16,1,64,256]{3,2,1,0:T(8,128)(2,1)}), bf16[16,1,64,256]{3,2,1,0:T(8,128)(2,1)S(1)}, u32[]{:S(2)}, u32[]{:S(2)}) async-start(bf16[16,1,64,256]{3,2,1,0:T(8,128)(2,1)} %convert_bitcast_fusion), calls=%async_computation.1 | async-start | bytes 1048576 | tf_op jit(solution)/shard_map/all_to_all | solution.py:13
  19.1 12.0 %all-to-all-done.1 = bf16[16,1,64,256]{3,2,1,0:T(8,128)(2,1)S(1)} async-done(((bf16[16,1,64,256]{3,2,1,0:T(8,128)(2,1)}), bf16[16,1,64,256]{3,2,1,0:T(8,128)(2,1)S(1)}, u32[]{:S(2)}, u32[]{:S(2)}) %all-to-all-start.1) | async-done | bytes 524320 | tf_op jit(solution)/shard_map/all_to_all | solution.py:13
  31.2 4.2 %all-to-all-start = ((bf16[16,2,64,256]{3,2,1,0:T(8,128)(2,1)}), bf16[16,2,64,256]{3,2,1,0:T(8,128)(2,1)S(1)}, u32[]{:S(2)}, u32[]{:S(2)}) async-start(bf16[16,2,64,256]{3,2,1,0:T(8,128)(2,1)} %pad_maximum_fusion.1), calls=%async_computation | async-start | bytes 2097152 | tf_op jit(solution)/shard_map/all_to_all | solution.py:13
  35.8 1.2 all_gather_reshape.7
  37.0 26.2 %all-to-all-done = bf16[16,2,64,256]{3,2,1,0:T(8,128)(2,1)S(1)} async-done(((bf16[16,2,64,256]{3,2,1,0:T(8,128)(2,1)}), bf16[16,2,64,256]{3,2,1,0:T(8,128)(2,1)S(1)}, u32[]{:S(2)}, u32[]{:S(2)}) %all-to-all-start) | async-done | bytes 1048608 | tf_op jit(solution)/shard_map/all_to_all | solution.py:13
  64.0 1.5 all_gather_reshape.6
  67.3 3.0 all-gather.10.cloned.1.call-done
  70.3 1.2 slice_bitcast_fusion
  73.0 19.4 %all-gather.8.cloned.1.call-done = bf16[2,1,256,1024]{3,2,1,0:T(8,128)(2,1)} async-done(((bf16[1,1,256,1024]{3,2,1,0:T(8,128)(2,1)}), bf16[2,1,256,1024]{3,2,1,0:T(8,128)(2,1)}) %all-gather.8.cloned.1.call-update) | async-done | bytes 1048592 | tf_op jit(solution)/shard_map/all_gather | solution.py:16
  92.4 1.5 copy.78
  93.9 33.8 %all-gather.6.cloned.1.call-done = bf16[2,2,256,1024]{3,2,1,0:T(8,128)(2,1)} async-done(((bf16[1,2,256,1024]{3,2,1,0:T(8,128)(2,1)}), bf16[2,2,256,1024]{3,2,1,0:T(8,128)(2,1)}) %all-gather.6.cloned.1.call-update) | async-done | bytes 2097168 | tf_op jit(solution)/shard_map/all_gather | solution.py:16
  127.7 3.7 %copy.82 = bf16[2,256,2,1024]{3,2,1,0:T(2,128)(2,1)S(1)} copy(bf16[2,256,2,1024]{3,1,0,2:T(8,128)(2,1)} %bitcast.89) | data formatting | bytes 4194304 | tf_op jit(solution)/shard_map/reshape | solution.py:16
  131.4 2.0 copy.89
  133.5 74.6 %all-gather.12.cloned.1.call-done = bf16[2176,2048]{1,0:T(8,128)(2,1)} async-done(((bf16[136,2048]{1,0:T(8,128)(2,1)}), bf16[2176,2048]{1,0:T(8,128)(2,1)}) %all-gather.12.cloned.1.call-update) | async-done | bytes 8912912 | tf_op jit(solution)/shard_map/all_gather | solution.py:41
  209.1 1.9 constant_dynamic-slice_fusion
  214.2 4.8 %fusion.15 = f32[2176,512]{1,0:T(8,128)S(1)} fusion(bf16[2176,2048]{1,0:T(8,128)(2,1)S(1)} %copy-done.6, bf16[512,2048]{1,0:T(8,128)(2,1)S(1)} %bitcast.99), kind=kOutput, calls=%fused_computation.45 | convolution fusion | flops 4563402752 | bytes 15466496 | tf_op jit(solution)/shard_map/dot_general | solution.py:20
  220.3 7.1 %convolution_convert_fusion = bf16[2048,2048]{1,0:T(8,128)(2,1)} fusion(bf16[2048,320]{1,0:T(8,128)(2,1)S(1)} %bitcast.104, bf16[64,2048]{0,1:T(8,128)(2,1)S(1)} %bitcast.97, bf16[256,2048]{0,1:T(8,128)(2,1)S(1)} %bitcast.92), kind=kOutput, calls=%fused_computation | convolution fusion | flops 2691170304 | bytes 11010048 | tf_op jit(solution)/shard_map/dot_general | solution.py:57
  227.4 2.1 copy.85
  229.5 1.7 copy.87
  231.9 1.4 copy.84
  233.3 2.6 copy.76
  235.9 3.2 fusion.13
  239.1 90.4 %reduce-scatter.2.cloned.1.call-done = bf16[128,2048]{1,0:T(8,128)(2,1)} async-done(((bf16[2048,2048]{1,0:T(8,128)(2,1)}), bf16[128,2048]{1,0:T(8,128)(2,1)}) %reduce-scatter.2.cloned.1.call-update) | async-done | bytes 524304 | tf_op jit(solution)/shard_map/reduce_scatter | solution.py:58
  (72 shorter events, 12.7 us)
Async XLA Ops:
  7.2 9.8 %copy-start.9 = (f32[64,256]{1,0:T(8,128)S(1)}, f32[64,256]{1,0:T(8,128)}, u32[]{:S(2)}) copy-start(f32[64,256]{1,0:T(8,128)} %param.16) | copy-start | bytes 196612
  7.2 9.9 %copy-start.7 = (f32[256,64]{0,1:T(8,128)S(1)}, f32[256,64]{0,1:T(8,128)}, u32[]{:S(2)}) copy-start(f32[256,64]{0,1:T(8,128)} %param.14) | copy-start | bytes 196612
  7.2 9.9 %copy-start.8 = (f32[256,64]{0,1:T(8,128)S(1)}, f32[256,64]{0,1:T(8,128)}, u32[]{:S(2)}) copy-start(f32[256,64]{0,1:T(8,128)} %param.15) | copy-start | bytes 196612
  7.2 9.8 %copy-start.10 = (f32[256]{0:T(256)S(1)}, f32[256]{0:T(256)}, u32[]{:S(2)}) copy-start(f32[256]{0:T(256)} %param.17) | copy-start | bytes 3076
  7.2 10.6 %copy-start.4 = (f32[16,256,64]{1,2,0:T(8,128)S(1)}, f32[16,256,64]{1,2,0:T(8,128)}, u32[]{:S(2)}) copy-start(f32[16,256,64]{1,2,0:T(8,128)} %param.11) | copy-start | bytes 3145732
  7.2 10.6 %copy-start.5 = (f32[16,256,64]{1,2,0:T(8,128)S(1)}, f32[16,256,64]{1,2,0:T(8,128)}, u32[]{:S(2)}) copy-start(f32[16,256,64]{1,2,0:T(8,128)} %param.12) | copy-start | bytes 3145732
  9.5 21.7 %all-to-all-start.1 = ((bf16[16,1,64,256]{3,2,1,0:T(8,128)(2,1)}), bf16[16,1,64,256]{3,2,1,0:T(8,128)(2,1)S(1)}, u32[]{:S(2)}, u32[]{:S(2)}) async-start(bf16[16,1,64,256]{3,2,1,0:T(8,128)(2,1)} %convert_bitcast_fusion), calls=%async_computation.1 | async-start | bytes 1048576 | tf_op jit(solution)/shard_map/all_to_all | solution.py:13
  16.9 53.4 %all-gather.10.cloned.1.call-start = ((), (), s32[]{:S(2)}) async-start(), calls=%async_computation.5 | async-start | bytes 1179648 | tf_op jit(solution)/shard_map/all_gather | solution.py:127
  31.2 32.1 %all-to-all-start = ((bf16[16,2,64,256]{3,2,1,0:T(8,128)(2,1)}), bf16[16,2,64,256]{3,2,1,0:T(8,128)(2,1)S(1)}, u32[]{:S(2)}, u32[]{:S(2)}) async-start(bf16[16,2,64,256]{3,2,1,0:T(8,128)(2,1)} %pad_maximum_fusion.1), calls=%async_computation | async-start | bytes 2097152 | tf_op jit(solution)/shard_map/all_to_all | solution.py:13
  35.3 57.1 %all-gather.8.cloned.1.call-start = ((), (), s32[]{:S(2)}) async-start(), calls=%async_computation.4 | async-start | bytes 1572864 | tf_op jit(solution)/shard_map/all_gather | solution.py:16
  37.0 90.7 %all-gather.6.cloned.1.call-start = ((), (), s32[]{:S(2)}) async-start(), calls=%async_computation.3 | async-start | bytes 3145728 | tf_op jit(solution)/shard_map/all_gather | solution.py:16
  63.2 2.4 copy-start.11
  63.2 2.5 copy-start.12
  63.2 2.6 copy-start.3
  65.6 142.4 %all-gather.12.cloned.1.call-start = ((), (), s32[]{:S(2)}) async-start(), calls=%async_computation.7 | async-start | bytes 9469952 | tf_op jit(solution)/shard_map/all_gather | solution.py:41
  67.0 262.5 %reduce-scatter.2.cloned.1.call-start = ((), (), s32[]{:S(2)}) async-start(), calls=%async_computation.6 | async-start | bytes 8912896 | tf_op jit(solution)/shard_map/reduce_scatter | solution.py:58
  73.0 147.3 %copy-start.1 = (bf16[1,64,8,256]{1,3,2,0:T(8,128)(2,1)}, bf16[1,64,8,256]{1,3,2,0:T(8,128)(2,1)S(1)}, u32[]{:S(2)}) copy-start(bf16[1,64,8,256]{1,3,2,0:T(8,128)(2,1)S(1)} %copy.81) | copy-start | bytes 786436
  209.1 4.2 %copy-start.6 = (bf16[2176,2048]{1,0:T(8,128)(2,1)S(1)}, bf16[2176,2048]{1,0:T(8,128)(2,1)}, u32[]{:S(2)}) copy-start(bf16[2176,2048]{1,0:T(8,128)(2,1)} %all-gather.12.cloned.1.call-done) | copy-start | bytes 26738692
  211.8 2.3 copy-start.2
  227.4 5.9 %copy-start = (bf16[2,2,256,1024]{3,2,1,0:T(8,128)(2,1)S(1)}, bf16[2,2,256,1024]{3,2,1,0:T(8,128)(2,1)}, u32[]{:S(2)}) copy-start(bf16[2,2,256,1024]{3,2,1,0:T(8,128)(2,1)} %all-gather.6.cloned.1.call-done) | copy-start | bytes 6291460
Sparse Core Ops, SparseCore 0:
  20.4 49.8 all-gather.9
  72.4 19.9 all-gather.7
  94.6 33.0 all-gather.5
  130.4 77.5 all-gather.11
  227.5 101.9 reduce-scatter.1
